TPU v7x, 32 devices: a whole 2x2x4 slice. The times are simulated.
32 devices in a mesh: grp: 2 (over y), fs: 4 (over z), tp: 4 (over x, core).
Axes of the slice: x: 2, y: 2, z: 4, core: 2. Of those that a mesh axis runs over, the one named last changes fastest.
Arguments:
- tokens: bfloat16 [4096, 2048], P(('grp', 'fs'), 'tp'), parts along dimension 0, may hold values from -16 to 16
- attn_gain: float32 [2048], replicated, may hold values from 0.1 to 1.9
- w_query: bfloat16 [2048, 1024], P('fs', 'tp'), may hold values from -0.125 to 0.125
- w_key: bfloat16 [2048, 1024], P('fs', 'tp'), may hold values from -0.125 to 0.125
- w_value: bfloat16 [2048, 2048], P('fs', 'tp'), may hold values from -0.125 to 0.125
- w_low: bfloat16 [2048, 32], replicated, may hold values from -0.125 to 0.125
- w_lift: bfloat16 [32, 1024], P(None, 'tp'), may hold values from -1 to 1
- decay_bias: float32 [1024], P('tp'), may hold values from -0.5 to 6
- head_gain: float32 [256], replicated, may hold values from 0.1 to 1.9
- w_out: bfloat16 [2048, 2048], P('tp', 'fs'), may hold values from -0.125 to 0.125
- ffn_gain: float32 [2048], replicated, may hold values from 0.1 to 1.9
- w_gate: bfloat16 [2048, 5632], P('fs', 'tp'), may hold values from -0.125 to 0.125
- w_up: bfloat16 [2048, 5632], P('fs', 'tp'), may hold values from -0.125 to 0.125
- w_down: bfloat16 [5632, 2048], P('tp', 'fs'), may hold values from -0.078125 to 0.078125
- final_gain: float32 [2048], P('tp'), may hold values from 0.1 to 1.9
Outputs:
- result: bfloat16 [4096, 2048], P(('grp', 'fs'), 'tp'), parts along dimension 0
There are 2 independent parts, one for each index of `grp`. A program takes and returns all parts, laid end to end along the dimension named above; an argument that names none is the same for every part. Nothing has to cross between parts.
All inputs are finite; a program needn't handle non-finite values.
Results may differ from a plain program's by a relative error of at most 0.015.
Values may be sent and summed in bfloat16 or wider, within the bound.
A program may use at most 64 MiB of HBM per device.

v0:
```python
import functools

import jax
import jax.numpy as jnp
from jax import lax
from jax.experimental import pallas as pl
from jax.experimental.pallas import tpu as pltpu
from jax.sharding import PartitionSpec as P

DK = 128
DV = 256
BLOCK = 64
epsilon = 1e-06
highest = lax.Precision.HIGHEST
MESH = pl.DeviceIdType.MESH
LANES = 128


def layer_kernel(
    sizes,
    tokens_ref,
    attn_gain_ref,
    w_low_ref,
    w_lift_ref,
    decay_bias_ref,
    head_gain_ref,
    ffn_gain_ref,
    final_gain_ref,
    w_query_ref,
    w_key_ref,
    w_value_ref,
    w_out_ref,
    w_gate_ref,
    w_up_ref,
    w_down_ref,
    result_ref,
    g_mix,
    g_out,
    g_gate,
    g_up,
    g_down,
    rows_all,
    normed,
    mix_rows,
    log_decay,
    mixed,
    state,
    partial_out,
    heard_out,
    first_all,
    gate_acc,
    up_acc,
    hidden,
    partial_down,
    heard_down,
    squares,
    down_send,
    down_recv,
    z_send,
    z_recv,
    y_send,
    y_recv,
    tp_send,
    tp_recv,
    local_sem,
):
    n, tp = sizes
    g, f, t = lax.axis_index("grp"), lax.axis_index("fs"), lax.axis_index("tp")
    rows, width = tokens_ref.shape
    features = width * tp
    f32 = jnp.float32

    messages, owned = [], []
    for group in (
        ((w_query_ref, w_key_ref, w_value_ref), g_mix),
        ((w_out_ref,), g_out),
        ((w_gate_ref,), g_gate),
        ((w_up_ref,), g_up),
    ):
        column = 0
        for w in group[0]:
            messages.append((w, group[1], 0, column, w.shape[1]))
            owned.append(messages[-1])
            column += w.shape[1]
    chunks = w_down_ref.shape[1] // LANES
    owned.append((w_down_ref, g_down, 0, 0, w_down_ref.shape[1]))
    first_down = len(messages)
    messages += [(w_down_ref, g_down, c * LANES, c * LANES, LANES) for c in range(chunks)]
    opening, middle = range(4), range(4, first_down)
    closing = range(first_down, len(messages))

    barrier = pltpu.get_barrier_semaphore()

    @pl.when(f > 0)
    def _():
        pl.semaphore_signal(barrier, inc=1, device_id=(g, f - 1, t), device_id_type=MESH)

    @pl.when(f < n - 1)
    def _():
        pl.semaphore_signal(barrier, inc=1, device_id=(g, f + 1, t), device_id_type=MESH)

    pl.semaphore_signal(barrier, inc=1, device_id=(1 - g, f, t), device_id_type=MESH)
    for d in range(1, tp):
        peer = lax.rem(t + d, tp)
        pl.semaphore_signal(barrier, inc=1, device_id=(g, f, peer), device_id_type=MESH)
    met = jnp.where(f > 0, 1, 0) + jnp.where(f < n - 1, 1, 0) + tp
    pl.semaphore_wait(barrier, met)

    def z_copy(m, way, step):
        w, held, start, column, columns = messages[m]
        owner = f - (step - 1) if way == 0 else f + (step - 1)
        part = w.shape[0] // 2
        half = pl.ds(pl.multiple_of(g * part, 16), part)
        at = held.at[owner, half, pl.ds(column, columns)]
        source = w.at[half, pl.ds(start, columns)] if step == 1 else at
        target = f + 1 if way == 0 else f - 1
        return pltpu.make_async_remote_copy(
            source, at, z_send.at[m, way, step], z_recv.at[m, way, step],
            device_id=(g, target, t), device_id_type=MESH,
        )

    def y_copy(m, way, step):
        w, held, _, column, columns = messages[m]
        part = w.shape[0] // 2
        half = pl.ds(pl.multiple_of(g * part, 16), part)
        at = held.at[f + step * (2 * way - 1), half, pl.ds(column, columns)]
        return pltpu.make_async_remote_copy(
            at, at, y_send.at[m, way, step], y_recv.at[m, way, step],
            device_id=(1 - g, f, t), device_id_type=MESH,
        )

    def gets(way, step):
        return f >= step if way == 0 else f + step < n

    def gives(way, step):
        if way == 0:
            return jnp.logical_and(f + 1 < n, f >= step - 1)
        return jnp.logical_and(f >= 1, f + step - 1 < n)

    def launch(m):
        for way in (0, 1):
            @pl.when(gives(way, 1))
            def _():
                z_copy(m, way, 1).start()

    def tick(m, step):
        for way in (0, 1):
            @pl.when(gets(way, step))
            def _():
                z_copy(m, way, step).wait_recv()
                y_copy(m, way, step).start()

            if step < n - 1:
                @pl.when(gives(way, step + 1))
                def _():
                    z_copy(m, way, step + 1).start()

    def arrived(m, way, step):
        y_copy(m, way, step).wait_recv()

    def all_arrived(m):
        for step in range(1, n):
            for way in (0, 1):
                @pl.when(gets(way, step))
                def _():
                    arrived(m, way, step)

    def tp_copy(kind, source, target, d, peer):
        return pltpu.make_async_remote_copy(
            source, target, tp_send.at[kind, d], tp_recv.at[kind, d],
            device_id=(g, f, peer), device_id_type=MESH,
        )

    def token_copy(d):
        return tp_copy(0, tokens_ref, rows_all.at[t], d, lax.rem(t + d, tp))

    def out_copy(d):
        peer = lax.rem(t + d, tp)
        return tp_copy(1, partial_out.at[peer], heard_out.at[d - 1], d, peer)

    def first_copy(d):
        return tp_copy(2, first_all.at[t], first_all.at[t], d, lax.rem(t + d, tp))

    def down_copy(d, c):
        peer = lax.rem(t + d, tp)
        part = pl.ds(c * (width // chunks), width // chunks)
        return pltpu.make_async_remote_copy(
            partial_down.at[peer, :, part], heard_down.at[d - 1, :, part],
            down_send.at[c, d], down_recv.at[c, d],
            device_id=(g, f, peer), device_id_type=MESH,
        )

    def square_copy(d):
        return tp_copy(3, squares.at[0], squares.at[d], d, lax.rem(t + d, tp))

    others = range(1, tp)
    for m in opening:
        launch(m)
    for d in others:
        token_copy(d).start()
    locals_ = [pltpu.make_async_copy(tokens_ref, rows_all.at[t], local_sem.at[0])]
    for index, (w, held, _, column, columns) in enumerate(owned):
        at = held.at[f, :, pl.ds(column, columns)]
        locals_.append(pltpu.make_async_copy(w, at, local_sem.at[index + 1]))
    for copy in locals_:
        copy.start()

    for step in range(1, max(n - 1, 2)):
        for m in opening:
            tick(m, step)
    for m in middle:
        launch(m)
    for copy in locals_:
        copy.wait()
    for d in others:
        token_copy(d).wait_recv()

    def normalize(source, gain_ref):
        total = jnp.zeros((rows, 1), f32)
        for p in range(tp):
            values = source[p].astype(f32)
            total += jnp.sum(values * values, axis=1, keepdims=True)
        factor = lax.rsqrt(total / features + epsilon)
        for p in range(tp):
            part = pl.ds(p * width, width)
            scaled = source[p].astype(f32) * factor * gain_ref[:, part]
            normed[:, part] = scaled.astype(jnp.bfloat16)

    def accumulate(held, acc):
        depth = held.shape[1]
        acc[...] = jnp.zeros_like(acc)

        def step(j, carry):
            columns = pl.ds(pl.multiple_of(j * depth, 128), depth)
            acc[...] += jnp.dot(normed[:, columns], held[j], preferred_element_type=f32)
            return carry

        lax.fori_loop(0, n, step, 0)

    normalize(rows_all, attn_gain_ref)
    low_rank = lax.dot_general(
        normed[...], w_low_ref[...], (((1,), (1,)), ((), ())), preferred_element_type=f32
    )
    lifted = jnp.dot(low_rank.astype(jnp.bfloat16), w_lift_ref[...], preferred_element_type=f32)
    log_decay[...] = jax.nn.log_sigmoid(lifted + decay_bias_ref[...]) / 16.0

    if n > 2:
        for m in opening:
            tick(m, n - 1)
    for m in range(3):
        all_arrived(m)
    mix_acc = up_acc.at[:, pl.ds(0, mix_rows.shape[1])]
    accumulate(g_mix, mix_acc)
    mix_rows[...] = mix_acc[...].astype(jnp.bfloat16)

    heads = mix_rows.shape[1] // (2 * DK + DV)
    at_row = lax.broadcasted_iota(jnp.int32, (BLOCK, BLOCK), 0)
    at_col = lax.broadcasted_iota(jnp.int32, (BLOCK, BLOCK), 1)
    causal = at_row >= at_col
    lower = causal.astype(f32)

    def dot(a, b, ca, cb):
        return lax.dot_general(
            a, b, (((ca,), (cb,)), ((), ())), precision=highest, preferred_element_type=f32
        )

    state[...] = jnp.zeros_like(state)

    def block_step(block, carry):
        here = pl.ds(pl.multiple_of(block * BLOCK, BLOCK), BLOCK)
        for h in range(heads):
            query = mix_rows[here, pl.ds(h * DK, DK)].astype(f32) * DK ** (-0.5)
            key = mix_rows[here, pl.ds((heads + h) * DK, DK)].astype(f32)
            value = mix_rows[here, pl.ds(2 * heads * DK + h * DV, DV)].astype(f32)
            cum = dot(lower, log_decay[here, pl.ds(h * DK, DK)], 1, 0)
            last = cum[BLOCK - 1 :, :]
            query_dec = query * jnp.exp(cum)
            key_dec = key * jnp.exp(-cum)
            scores = jnp.where(causal, dot(query_dec, key_dec, 1, 1), 0.0)
            held = state[h]
            out = dot(scores, value, 1, 0) + dot(query_dec, held, 1, 0)
            decay = jnp.transpose(jnp.broadcast_to(jnp.exp(last), (DK, DK)))
            decay = jnp.concatenate([decay] * (DV // DK), axis=1)
            state[h] = decay * held + dot(key * jnp.exp(last - cum), value, 0, 0)
            factor = lax.rsqrt(jnp.mean(out * out, axis=1, keepdims=True) + epsilon)
            mixed[here, pl.ds(h * DV, DV)] = (out * factor * head_gain_ref[...]).astype(jnp.bfloat16)
        return carry

    gate_at, up_at = middle
    blocks = rows // BLOCK
    lax.fori_loop(0, blocks // 2, block_step, 0)
    if n > 2:
        tick(gate_at, 1)
    lax.fori_loop(blocks // 2, blocks, block_step, 0)
    all_arrived(3)

    def block_place(j, columns):
        return j * columns // width, pl.ds(pl.multiple_of(lax.rem(j * columns, width), 128), columns)

    def out_step(j, carry):
        p, part = block_place(j, g_out.shape[2])
        terms = jnp.dot(mixed[...], g_out[j], preferred_element_type=f32)
        partial_out[p, :, part] = terms.astype(jnp.bfloat16)
        return carry

    lax.fori_loop(0, n, out_step, 0)
    for d in others:
        out_copy(d).start()
    if n > 2:
        tick(up_at, 1)
    if n > 3:
        tick(gate_at, 2)
    for d in others:
        out_copy(d).wait_recv()
    total = partial_out[t].astype(f32)
    for d in others:
        total += heard_out[d - 1].astype(f32)
    first_all[t] = (rows_all[t].astype(f32) + total).astype(jnp.bfloat16)
    for d in others:
        first_copy(d).start()
    for step in range(2, n - 1):
        if step > 2:
            tick(gate_at, step)
        tick(up_at, step)
    for m in closing:
        launch(m)
    for d in others:
        first_copy(d).wait_recv()
    normalize(first_all, ffn_gain_ref)
    tick(gate_at, n - 1)
    all_arrived(gate_at)
    accumulate(g_gate, gate_acc)
    tick(up_at, n - 1)
    for m in closing:
        tick(m, 1)
    all_arrived(up_at)
    accumulate(g_up, up_acc)
    gate = gate_acc[...]
    hidden[...] = (gate / (1.0 + jnp.exp(-gate)) * up_acc[...]).astype(jnp.bfloat16)
    eager = g_down.shape[2] == width

    def down_block(j, c):
        place = j * g_down.shape[2] + c * LANES
        p, part = place // width, pl.ds(pl.multiple_of(lax.rem(place, width), LANES), LANES)
        columns = pl.ds(c * LANES, LANES)
        terms = jnp.dot(hidden[...], g_down[j, :, columns], preferred_element_type=f32)
        partial_down[p, :, part] = terms.astype(jnp.bfloat16)
        if eager:
            for d in others:
                @pl.when(j == lax.rem(t + d, tp))
                def _():
                    down_copy(d, c).start()

    for c in range(chunks):
        down_block(f, c)
    for step in range(1, n):
        if step > 1:
            for m in closing:
                tick(m, step)
        for c, m in enumerate(closing):
            def from_way(way, carry):
                j = f + step * (2 * way - 1)

                @pl.when(jnp.logical_and(j >= 0, j < n))
                def _():
                    y_copy(m, way, step).wait_recv()
                    down_block(j, c)

                return carry

            lax.fori_loop(0, 2, from_way, 0)
    if not eager:
        for d in others:
            for c in range(chunks):
                down_copy(d, c).start()
    for d in others:
        for c in range(chunks):
            down_copy(d, c).wait_recv()
    second = partial_down[t].astype(f32)
    for d in others:
        second += heard_down[d - 1].astype(f32)
    second = first_all[t].astype(f32) + second
    ones = jnp.ones((8, width), f32)
    squares[0] = dot(ones, second * second, 1, 1)
    for d in others:
        square_copy(d).start()
    for d in others:
        square_copy(d).wait_recv()
    whole = squares[0]
    for d in others:
        whole += squares[d]
    factor = lax.rsqrt(jnp.transpose(whole) / features + epsilon)[:, :1]
    result_ref[...] = (second * factor * final_gain_ref[...]).astype(jnp.bfloat16)

    for m in range(len(messages)):
        for step in range(1, n):
            for way in (0, 1):
                @pl.when(gives(way, step))
                def _():
                    z_copy(m, way, step).wait_send()

                @pl.when(gets(way, step))
                def _():
                    y_copy(m, way, step).wait_send()
    for d in others:
        for copy in (token_copy, out_copy, first_copy, square_copy):
            copy(d).wait_send()
        for c in range(chunks):
            down_copy(d, c).wait_send()


def body(
    sizes, tokens, attn_gain, w_query, w_key, w_value, w_low, w_lift, decay_bias, head_gain,
    w_out, ffn_gain, w_gate, w_up, w_down, final_gain,
):
    n, tp = sizes
    rows, width = tokens.shape
    bf16, f32 = jnp.bfloat16, jnp.float32
    units, keys, values = w_gate.shape[1], w_query.shape[1], w_value.shape[1]
    mix_width = 2 * keys + values
    held = [pltpu.VMEM((n, w_query.shape[0], mix_width), bf16)]
    held += [pltpu.VMEM((n, *w.shape), bf16) for w in (w_out, w_gate, w_up, w_down)]
    chunks = w_down.shape[1] // LANES
    messages = 6 + chunks
    dma = pltpu.SemaphoreType.DMA
    anywhere = pl.BlockSpec(memory_space=pl.ANY)
    inside = pl.BlockSpec(memory_space=pltpu.VMEM)
    return pl.pallas_call(
        functools.partial(layer_kernel, sizes),
        name="layer",
        out_shape=jax.ShapeDtypeStruct((rows, width), bf16),
        in_specs=[anywhere] + [inside] * 7 + [anywhere] * 7,
        out_specs=inside,
        scratch_shapes=held + [
            pltpu.VMEM((tp, rows, width), bf16),
            pltpu.VMEM((rows, width * tp), bf16),
            pltpu.VMEM((rows, mix_width), bf16),
            pltpu.VMEM((rows, keys), f32),
            pltpu.VMEM((rows, values), bf16),
            pltpu.VMEM((keys // DK, DK, DV), f32),
            pltpu.VMEM((tp, rows, width), bf16),
            pltpu.VMEM((tp - 1, rows, width), bf16),
            pltpu.VMEM((tp, rows, width), bf16),
            pltpu.VMEM((rows, units), f32),
            pltpu.VMEM((rows, units), f32),
            pltpu.VMEM((rows, units), bf16),
            pltpu.VMEM((tp, rows, width), bf16),
            pltpu.VMEM((tp - 1, rows, width), bf16),
            pltpu.VMEM((tp, 8, rows), f32),
            dma((chunks, tp)),
            dma((chunks, tp)),
            dma((messages, 2, n)),
            dma((messages, 2, n)),
            dma((messages, 2, n)),
            dma((messages, 2, n)),
            dma((4, tp)),
            dma((4, tp)),
            dma((8,)),
        ],
        compiler_params=pltpu.CompilerParams(
            collective_id=0, has_side_effects=True, vmem_limit_bytes=63 * 1024 * 1024
        ),
    )(
        tokens, attn_gain[None], w_low.T, w_lift, decay_bias[None], head_gain[None],
        ffn_gain[None], final_gain[None], w_query, w_key, w_value, w_out, w_gate, w_up, w_down,
    )


def solution(mesh):
    sizes = (mesh.shape["fs"], mesh.shape["tp"])
    return jax.shard_map(
        functools.partial(body, sizes),
        mesh=mesh,
        in_specs=(
            P(("grp", "fs"), "tp"),
            P(),
            P("fs", "tp"),
            P("fs", "tp"),
            P("fs", "tp"),
            P(),
            P(None, "tp"),
            P("tp"),
            P(),
            P("tp", "fs"),
            P(),
            P("fs", "tp"),
            P("fs", "tp"),
            P("tp", "fs"),
            P("tp"),
        ),
        out_specs=P(("grp", "fs"), "tp"),
        check_vma=False,
    )
```

profile of v0, /device:TPU:0, one launch (start us, length us, event | category | flops | bytes accessed | tf_op | source)
XLA Modules:
  0.0 232.3 jit_solution(6496554131433043323)
XLA Ops:
  0.0 230.4 %layer.1 = bf16[512,512]{1,0:T(8,128)(2,1)} custom-call(bf16[512,512]{1,0:T(8,128)(2,1)} %tokens_ref.1, f32[1,2048]{1,0:T(1,128)} %bitcast.7, bf16[32,2048]{1,0:T(8,128)(2,1)} %bitcast.6, bf16[32,256]{1,0:T(8,128)(2,1)} %w_lift_ref.1, f32[1,256]{1,0:T(1,128)} %bitcast.10, f32[1,256]{1,0:T(1,128)} %bitcast.11, f32[1,2048]{1,0:T(1,128)} %bitcast.8, ...), custom_call_target="tpu_custom_call" | custom-call | tf_op jit(solution)/shard_map/layer/pallas_call | solution.py:428
  230.4 1.9 copy.17
where the time goes:
time: 232 us
  Pallas kernels  230 us (99%)
    pallas_call x1, Pallas kernels, body(): pl.pallas_call(functools.partial(layer_kernel, sizes), name='layer', out_...  230 us

commit v1 on v0

v1 whole, which is shorter than its diff:
```python
import functools

import jax
import jax.numpy as jnp
from jax import lax
from jax.experimental import pallas as pl
from jax.experimental.pallas import tpu as pltpu
from jax.sharding import PartitionSpec as P

DK = 128
DV = 256
BLOCK = 64
epsilon = 1e-06
highest = lax.Precision.HIGHEST
MESH = pl.DeviceIdType.MESH
LANES = 128
HALVES = 2


def unit_chunks(units):
    if units % LANES:
        return [(0, units)]
    tiles = units // LANES
    pieces = [-(-tiles // 3) + (-(-tiles // 3)) % 2] * 3
    chunks, start = [], 0
    for piece in pieces:
        size = min(piece, tiles - start)
        if size > 0:
            chunks.append((start * LANES, size * LANES))
            start += size
    return chunks


def down_columns(columns):
    return 2 * LANES if columns % (2 * LANES) == 0 else LANES


def layer_kernel(
    sizes,
    tokens_ref,
    attn_gain_ref,
    w_low_ref,
    w_lift_ref,
    decay_bias_ref,
    head_gain_ref,
    ffn_gain_ref,
    final_gain_ref,
    w_query_ref,
    w_key_ref,
    w_value_ref,
    w_out_ref,
    w_gate_ref,
    w_up_ref,
    w_down_ref,
    result_ref,
    g_mix,
    g_out,
    g_gate,
    g_up,
    g_down,
    rows_all,
    normed,
    mix_rows,
    log_decay,
    mixed,
    state,
    partial_out,
    sib_out,
    far_out,
    first_all,
    hidden,
    partial_down,
    sib_down,
    far_down,
    sum_out,
    sum_in,
    second,
    squares,
    z_send,
    z_recv,
    y_send,
    y_recv,
    e_send,
    e_recv,
    ag_send,
    ag_recv,
    rs_send,
    rs_recv,
    dd_send,
    dd_recv,
    dx_send,
    dx_recv,
    guest_send,
    guest_recv,
    back_send,
    back_recv,
    sq_send,
    sq_recv,
    local_sem,
):
    n, tp = sizes
    chips = tp // 2
    g, f, t = lax.axis_index("grp"), lax.axis_index("fs"), lax.axis_index("tp")
    chip, core = t // 2, lax.rem(t, 2)
    sibling = t + 1 - 2 * core
    rows, width = tokens_ref.shape
    features = width * tp
    f32, bf16 = jnp.float32, jnp.bfloat16
    inner = jnp.logical_and(f > 0, f < n - 1)
    outer = jnp.logical_not(inner)
    has_guest = jnp.logical_or(f == 1, f == n - 2)
    guests = jnp.where(has_guest, 1, 0)
    guest_plane = jnp.where(f == 1, 0, n - 1)
    host_plane = jnp.where(f == 0, 1, n - 2)
    near = jnp.where(2 * f < n, 0, 1)
    far = 1 - near

    messages = []
    column = 0
    for w in (w_query_ref, w_key_ref, w_value_ref):
        messages.append((w, g_mix, 0, column, w.shape[1]))
        column += w.shape[1]
    messages.append((w_out_ref, g_out, 0, 0, w_out_ref.shape[1]))
    n_mix = len(messages)
    qkv, outs = range(3), range(3, 4)
    chunks = unit_chunks(w_gate_ref.shape[1])
    ffn_groups = []
    for start, size in chunks:
        ffn_groups.append((len(messages), len(messages) + 1))
        messages.append((w_gate_ref, g_gate, start, start, size))
        messages.append((w_up_ref, g_up, start, start, size))
    cols = w_down_ref.shape[1]
    dc = down_columns(cols)
    pieces = cols // dc
    down_at = len(messages)
    for c in range(pieces):
        messages.append((w_down_ref, g_down, c * dc, c * dc, dc))
    down_groups = [(down_at + c,) for c in range(pieces)]
    total_messages = len(messages)

    def is_ffn(m):
        return m >= n_mix

    def comes_whole(m, step):
        return step == 1 and (is_ffn(m) or m in qkv)

    def steps_of(m):
        return n - 2 if is_ffn(m) else n - 1

    barrier = pltpu.get_barrier_semaphore()

    @pl.when(f > 0)
    def _():
        pl.semaphore_signal(barrier, inc=1, device_id=(g, f - 1, t), device_id_type=MESH)

    @pl.when(f < n - 1)
    def _():
        pl.semaphore_signal(barrier, inc=1, device_id=(g, f + 1, t), device_id_type=MESH)

    pl.semaphore_signal(barrier, inc=1, device_id=(1 - g, f, t), device_id_type=MESH)
    for d in range(1, tp):
        peer = lax.rem(t + d, tp)
        pl.semaphore_signal(barrier, inc=1, device_id=(g, f, peer), device_id_type=MESH)
    met = jnp.where(f > 0, 1, 0) + jnp.where(f < n - 1, 1, 0) + tp
    pl.semaphore_wait(barrier, met)

    def half_of(w, which):
        part = w.shape[0] // 2
        return pl.ds(pl.multiple_of(which * part, 16), part)

    def toward(way):
        return f + 1 - 2 * way

    def z_copy(m, way, step):
        w, held, start, column, columns = messages[m]
        owner = f + (step - 1) * (2 * way - 1)
        half = half_of(w, g)
        at = held.at[owner, half, pl.ds(column, columns)]
        source = w.at[half, pl.ds(start, columns)] if step == 1 else at
        return pltpu.make_async_remote_copy(
            source, at, z_send.at[m, way, step], z_recv.at[m, way, step],
            device_id=(g, toward(way), t), device_id_type=MESH,
        )

    def e_copy(m, way, owner):
        w, held, start, column, columns = messages[m]
        half = half_of(w, 1 - g)
        at = held.at[owner, half, pl.ds(column, columns)]
        return pltpu.make_async_remote_copy(
            w.at[half, pl.ds(start, columns)], at, e_send.at[m, way], e_recv.at[m, way],
            device_id=(g, toward(way), t), device_id_type=MESH,
        )

    def y_copy(m, way, step):
        w, held, _, column, columns = messages[m]
        at = held.at[f + step * (2 * way - 1), half_of(w, g), pl.ds(column, columns)]
        return pltpu.make_async_remote_copy(
            at, at, y_send.at[m, way, step], y_recv.at[m, way, step],
            device_id=(1 - g, f, t), device_id_type=MESH,
        )

    def gets(m, way, step):
        j = f + step * (2 * way - 1)
        there = jnp.logical_and(j >= 0, j < n)
        return jnp.logical_and(there, inner) if is_ffn(m) else there

    def gives(m, way, step):
        j = f + (step - 1) * (2 * way - 1)
        there = jnp.logical_and(j >= 0, j < n)
        to = toward(way)
        low, high = (1, n - 2) if is_ffn(m) else (0, n - 1)
        return jnp.logical_and(there, jnp.logical_and(to >= low, to <= high))

    def gives_whole(way):
        return f == jnp.where(way == 0, 0, n - 1)

    def gets_whole(way):
        return f == jnp.where(way == 0, 1, n - 2)

    def launch(group, way):
        for m in group:
            @pl.when(gives(m, way, 1))
            def _():
                z_copy(m, way, 1).start()

    def complete(group):
        for way in (0, 1):
            for m in group:
                @pl.when(gives_whole(way))
                def _():
                    e_copy(m, way, f).start()

    def tick(group, way, step):
        for m in group:
            if step > steps_of(m):
                continue

            @pl.when(gets(m, way, step))
            def _():
                received(m, way, step).wait_recv()
                if comes_whole(m, step):
                    @pl.when(jnp.logical_not(gets_whole(way)))
                    def _():
                        y_copy(m, way, step).start()
                else:
                    y_copy(m, way, step).start()

            if step < steps_of(m):
                @pl.when(gives(m, way, step + 1))
                def _():
                    z_copy(m, way, step + 1).start()

    def received(m, way, step):
        w, held, start, column, columns = messages[m]
        at = held.at[f + step * (2 * way - 1), half_of(w, g), pl.ds(column, columns)]
        return pltpu.make_async_remote_copy(
            at, at, z_send.at[m, way, step], z_recv.at[m, way, step],
            device_id=(g, toward(way), t), device_id_type=MESH,
        )

    def arrived(m, way, step):
        if comes_whole(m, step):
            whole = gets_whole(way)

            @pl.when(whole)
            def _():
                e_copy(m, way, f + 2 * way - 1).wait_recv()

            @pl.when(jnp.logical_not(whole))
            def _():
                y_copy(m, way, step).wait_recv()
        else:
            y_copy(m, way, step).wait_recv()

    def all_arrived(group):
        for m in group:
            for step in range(1, steps_of(m) + 1):
                for way in (0, 1):
                    @pl.when(gets(m, way, step))
                    def _():
                        arrived(m, way, step)

    def peer_of(e):
        return 2 * lax.rem(chip + e, chips) + core

    def from_of(e):
        return 2 * lax.rem(chip - e + chips, chips) + core

    def tp_copy(source, target, send, recv, peer):
        return pltpu.make_async_remote_copy(
            source, target, send, recv, device_id=(g, f, peer), device_id_type=MESH
        )

    def ag_copy(kind, slot, source, target, peer):
        return tp_copy(source, target, ag_send.at[kind, slot], ag_recv.at[kind, slot], peer)

    others = range(1, tp)
    beyond = range(1, chips)

    def gather_out(kind, source, at):
        for e in beyond:
            ag_copy(kind, e, source, at(t), peer_of(e)).start()
        ag_copy(kind, 0, source, at(t), sibling).start()

    def gather_forward(kind, at):
        for e in beyond:
            came = at(from_of(e))
            ag_copy(kind, e, came, came, peer_of(e)).wait_recv()
            ag_copy(kind, chips - 1 + e, came, came, sibling).start()

    def gather_wait(kind, at):
        ag_copy(kind, 0, at(sibling), at(sibling), sibling).wait_recv()
        for e in beyond:
            came = at(from_of(e) + 1 - 2 * core)
            ag_copy(kind, chips - 1 + e, came, came, sibling).wait_recv()

    def gather_drain(kind, at):
        for slot in range(tp - 1):
            ag_copy(kind, slot, at(t), at(t), sibling).wait_send()

    def rows_of(h):
        return pl.ds(h * (rows // HALVES), rows // HALVES)

    def token_at(p):
        return rows_all.at[p]

    def first_at(r, h):
        return lambda p: first_all.at[r, p, rows_of(h)]

    def ag_kind(r, h):
        return 1 + r * HALVES + h

    def square_copy(d):
        peer = lax.rem(t + d, tp)
        return tp_copy(squares.at[0], squares.at[d], sq_send.at[d], sq_recv.at[d], peer)

    ahead = ffn_groups + down_groups
    ways = {"near": (near, n // 2 - 1), "far": (far, n - 2)}
    launched, ticked = set(), set()

    def send_own(i):
        if i < len(ahead) and i not in launched:
            launched.add(i)
            for way in (0, 1):
                launch(ahead[i], way)

    def relay(i, which, step=None):
        if i >= len(ahead):
            return
        way, top = ways[which]
        for s in range(1, top + 1):
            if step in (None, s) and (i, which, s) not in ticked:
                ticked.add((i, which, s))
                tick(ahead[i], way, s)

    def relayed(i):
        send_own(i)
        relay(i, "near")
        relay(i, "far")

    first_down = len(ffn_groups)

    def pump(k):
        for act in plan.get(k, ()):
            act()

    last_unit = len(ffn_groups) - 1
    plan = {
        -1: [lambda: send_own(0), lambda: send_own(1)],
        0: [lambda: relay(0, "near")],
        1: [lambda: relay(0, "far", 1)],
        2: [lambda: send_own(2), lambda: relay(1, "far", 1)],
        3: [lambda: relay(1, "near"), lambda: relay(0, "far"), lambda: send_own(3)],
        4: [lambda: relay(2, "far", 1)],
        5: [lambda: relay(2, "near"), lambda: send_own(4), lambda: relay(1, "far")],
        6: [lambda: relay(3, "far", 1)],
        7: [lambda: relay(2, "far")],
        8: [lambda: relay(4, "far", 1), lambda: relay(3, "near")],
        9: [lambda: relay(3, "far")],
        10: [lambda: relay(4, "near")],
    }

    def last_step(way):
        return jnp.where(way == 0, f, n - 1 - f)

    def after(step, way, group):
        @pl.when(last_step(way) == step)
        def _():
            launch(group, way)

    for way in (0, 1):
        launch(qkv, way)
        after(0, way, outs)

    @pl.when(outer)
    def _():
        complete(qkv)
        for group in ffn_groups:
            for way in (0, 1):
                launch(group, way)
            if group != ffn_groups[-1]:
                complete(group)

    gather_out(0, tokens_ref, token_at)
    locals_ = [pltpu.make_async_copy(tokens_ref, rows_all.at[t], local_sem.at[0])]
    own = [messages[m] for m in range(n_mix)]
    for index, (w, held, start, column, columns) in enumerate(own):
        at = held.at[f, :, pl.ds(column, columns)]
        locals_.append(pltpu.make_async_copy(w, at, local_sem.at[1 + index]))
    inner_locals = []
    for index, (w, held) in enumerate(((w_gate_ref, g_gate), (w_up_ref, g_up), (w_down_ref, g_down))):
        inner_locals.append(pltpu.make_async_copy(w, held.at[f], local_sem.at[1 + n_mix + index]))
    for copy in locals_:
        copy.start()

    @pl.when(inner)
    def _():
        for copy in inner_locals:
            copy.start()

    for step in range(1, n):
        for m in qkv:
            for way in (0, 1):
                tick((m,), way, step)
        for way in (0, 1):
            after(step, way, outs)
        if step == 1:
            gather_forward(0, token_at)
    for step in range(1, n // 2):
        tick(outs, near, step)
    pl.when(inner)(lambda: pump(-1))

    @pl.when(inner)
    def _():
        for copy in inner_locals:
            copy.wait()

    for copy in locals_:
        copy.wait()
    gather_wait(0, token_at)

    def normalize(source, slot, gain_ref, at):
        total = jnp.zeros((at.size, 1), f32)
        for p in range(tp):
            values = source[p, at].astype(f32)
            total += jnp.sum(values * values, axis=1, keepdims=True)
        factor = lax.rsqrt(total / features + epsilon)
        for p in range(tp):
            part = pl.ds(p * width, width)
            scaled = source[p, at].astype(f32) * factor * gain_ref[:, part]
            normed[slot, at, part] = scaled.astype(bf16)

    def product(lhs, held, at, size):
        block = held[:, :, pl.ds(at, size)]
        block = block.reshape(block.shape[0] * block.shape[1], size)
        return jnp.dot(lhs, block, preferred_element_type=f32)

    for h in range(HALVES):
        normalize(rows_all, 0, attn_gain_ref, rows_of(h))
    low_rank = lax.dot_general(
        normed[0], w_low_ref[...], (((1,), (1,)), ((), ())), preferred_element_type=f32
    )
    lifted = jnp.dot(low_rank.astype(bf16), w_lift_ref[...], preferred_element_type=f32)
    log_decay[...] = jax.nn.log_sigmoid(lifted + decay_bias_ref[...]) / 16.0

    all_arrived(qkv)
    tick(outs, far, 1)
    mix_block = 2 * LANES if mix_rows.shape[1] % (2 * LANES) == 0 else LANES

    def mix_step(i, carry):
        at = pl.multiple_of(i * mix_block, LANES)
        mix_rows[:, pl.ds(at, mix_block)] = product(normed[0], g_mix, at, mix_block).astype(bf16)
        return carry

    lax.fori_loop(0, mix_rows.shape[1] // mix_block, mix_step, 0)
    for step in range(2, n - 1):
        tick(outs, far, step)

    pl.when(inner)(lambda: pump(0))
    heads = mix_rows.shape[1] // (2 * DK + DV)
    at_row = lax.broadcasted_iota(jnp.int32, (BLOCK, BLOCK), 0)
    at_col = lax.broadcasted_iota(jnp.int32, (BLOCK, BLOCK), 1)
    causal = at_row >= at_col
    lower = causal.astype(f32)

    def dot(a, b, ca, cb):
        return lax.dot_general(
            a, b, (((ca,), (cb,)), ((), ())), precision=highest, preferred_element_type=f32
        )

    state[...] = jnp.zeros_like(state)

    def block_step(block, carry):
        here = pl.ds(pl.multiple_of(block * BLOCK, BLOCK), BLOCK)
        for h in range(heads):
            query = mix_rows[here, pl.ds(h * DK, DK)].astype(f32) * DK ** (-0.5)
            key = mix_rows[here, pl.ds((heads + h) * DK, DK)].astype(f32)
            value = mix_rows[here, pl.ds(2 * heads * DK + h * DV, DV)].astype(f32)
            cum = dot(lower, log_decay[here, pl.ds(h * DK, DK)], 1, 0)
            last = cum[BLOCK - 1 :, :]
            query_dec = query * jnp.exp(cum)
            key_dec = key * jnp.exp(-cum)
            scores = jnp.where(causal, dot(query_dec, key_dec, 1, 1), 0.0)
            held = state[h]
            out = dot(scores, value, 1, 0) + dot(query_dec, held, 1, 0)
            decay = jnp.transpose(jnp.broadcast_to(jnp.exp(last), (DK, DK)))
            decay = jnp.concatenate([decay] * (DV // DK), axis=1)
            state[h] = decay * held + dot(key * jnp.exp(last - cum), value, 0, 0)
            factor = lax.rsqrt(jnp.mean(out * out, axis=1, keepdims=True) + epsilon)
            mixed[here, pl.ds(h * DV, DV)] = (out * factor * head_gain_ref[...]).astype(bf16)
        return carry

    blocks = rows // BLOCK
    lax.fori_loop(0, blocks // 2, block_step, 0)
    pl.when(inner)(lambda: pump(1))
    lax.fori_loop(blocks // 2, blocks, block_step, 0)
    tick(outs, far, n - 1)
    all_arrived(outs)

    def block_place(place, size):
        return place // width, pl.ds(pl.multiple_of(lax.rem(place, width), LANES), size)

    def rs_copy(h, slot, source, target, peer):
        return tp_copy(source, target, rs_send.at[h, slot], rs_recv.at[h, slot], peer)

    def sib_copy(h, c):
        return rs_copy(
            h, c, partial_out.at[2 * c + 1 - core, rows_of(h)], sib_out.at[c, rows_of(h)], sibling
        )

    def far_copy(h, e):
        return rs_copy(
            h, chips - 1 + e, partial_out.at[peer_of(e), rows_of(h)],
            far_out.at[e - 1, rows_of(h)], peer_of(e),
        )

    out_cols = g_out.shape[2]
    for h in range(HALVES):
        def out_step(j, carry):
            p, part = block_place(j * out_cols, out_cols)
            terms = jnp.dot(mixed[rows_of(h), :], g_out[j], preferred_element_type=f32)
            partial_out[p, rows_of(h), part] = terms.astype(bf16)
            return carry

        lax.fori_loop(0, n, out_step, 0)
        for c in range(chips):
            sib_copy(h, c).start()
    for h in range(HALVES):
        for c in range(chips):
            sib_copy(h, c).wait_recv()
        for e in beyond:
            there = lax.rem(chip + e, chips)
            p = peer_of(e)
            pair = partial_out[p, rows_of(h)].astype(f32) + sib_out[there, rows_of(h)].astype(f32)
            partial_out[p, rows_of(h)] = pair.astype(bf16)
            far_copy(h, e).start()
    pl.when(inner)(lambda: pump(2))

    def guest_copy(h):
        at = rows_of(h)
        return pltpu.make_async_remote_copy(
            first_all.at[0, t, at], first_all.at[1, t, at], guest_send.at[h], guest_recv.at[h],
            device_id=(g, host_plane, t), device_id_type=MESH,
        )

    for h in range(HALVES):
        for e in beyond:
            far_copy(h, e).wait_recv()
        total = partial_out[t, rows_of(h)].astype(f32) + sib_out[chip, rows_of(h)].astype(f32)
        for e in beyond:
            total += far_out[e - 1, rows_of(h)].astype(f32)
        first_all[0, t, rows_of(h)] = (rows_all[t, rows_of(h)].astype(f32) + total).astype(bf16)

        @pl.when(inner)
        def _():
            gather_out(ag_kind(0, h), first_all.at[0, t, rows_of(h)], first_at(0, h))

        @pl.when(outer)
        def _():
            guest_copy(h).start()

    @pl.when(outer)
    def _():
        complete(ffn_groups[-1])
        for way in (0, 1):
            for group in down_groups:
                launch(group, way)
        for group in down_groups:
            complete(group)

    def units_step(r, start, size):
        gate = product(normed[r], g_gate, start, size)
        up = product(normed[r], g_up, start, size)
        hidden[r, :, pl.ds(start, size)] = (gate / (1.0 + jnp.exp(-gate)) * up).astype(bf16)

    def ffn_chunk(ci, r):
        start, size = chunks[ci]
        block = 2 * LANES
        whole = size // block

        def step(i, carry):
            units_step(r, pl.multiple_of(start + i * block, LANES), block)
            return carry

        lax.fori_loop(0, whole, step, 0)
        if size % block:
            units_step(r, start + whole * block, size % block)

    def guest_gather():
        for h in range(HALVES):
            guest_copy(h).wait_recv()
            gather_out(ag_kind(1, h), first_all.at[1, t, rows_of(h)], first_at(1, h))

    def guest_forward():
        for h in range(HALVES):
            gather_forward(ag_kind(1, h), first_at(1, h))

    def guest_ready():
        for h in range(HALVES):
            gather_wait(ag_kind(1, h), first_at(1, h))
            normalize(first_all.at[1], 1, ffn_gain_ref, rows_of(h))

    def place_of(j, c):
        p, part = block_place(j * cols + c * dc, dc)
        return p, part

    def dd_copy(r, j, c):
        p, part = place_of(j, c)
        return tp_copy(
            partial_down.at[r, p, :, part], sib_down.at[r, p // 2, :, part],
            dd_send.at[j * pieces + c, r], dd_recv.at[j * pieces + c, r], sibling,
        )

    def dx_copy(r, j, c, e):
        p, part = place_of(j, c)
        return tp_copy(
            partial_down.at[r, p, :, part], far_down.at[r, e - 1, :, part],
            dx_send.at[j * pieces + c, r, e - 1], dx_recv.at[j * pieces + c, r, e - 1],
            2 * (p // 2) + core,
        )

    def sets(act):
        def one(i, carry):
            act(guests - i)
            return carry

        lax.fori_loop(0, 1 + guests, one, 0)

    def down_compute(j, c):
        p, part = place_of(j, c)

        def act(r):
            terms = jnp.dot(hidden[r], g_down[j, :, pl.ds(c * dc, dc)], preferred_element_type=f32)
            partial_down[r, p, :, part] = terms.astype(bf16)

            @pl.when(lax.rem(p, 2) != core)
            def _():
                dd_copy(r, j, c).start()

        sets(act)

    def down_pass(j, c):
        p, part = place_of(j, c)

        @pl.when(jnp.logical_and(lax.rem(p, 2) == core, p // 2 != chip))
        def _():
            def act(r):
                dd_copy(r, j, c).wait_recv()
                pair = partial_down[r, p, :, part].astype(f32)
                pair += sib_down[r, p // 2, :, part].astype(f32)
                partial_down[r, p, :, part] = pair.astype(bf16)
                for e in beyond:
                    @pl.when(lax.rem(chip + e, chips) == p // 2)
                    def _():
                        dx_copy(r, j, c, e).start()

            sets(act)

    def down_total(r):
        for j in range(n):
            for c in range(pieces):
                @pl.when((j * cols + c * dc) // width == t)
                def _():
                    dd_copy(r, j, c).wait_recv()
                    for e in beyond:
                        dx_copy(r, j, c, e).wait_recv()
        total = partial_down[r, t].astype(f32) + sib_down[r, chip].astype(f32)
        for e in beyond:
            total += far_down[r, e - 1].astype(f32)
        return total

    def back_copy():
        return pltpu.make_async_remote_copy(
            sum_out, sum_in, back_send, back_recv,
            device_id=(g, guest_plane, t), device_id_type=MESH,
        )

    @pl.when(inner)
    def _():
        pump(3)
        for h in range(HALVES):
            gather_forward(ag_kind(0, h), first_at(0, h))
        for h in range(HALVES):
            gather_wait(ag_kind(0, h), first_at(0, h))
            normalize(first_all.at[0], 0, ffn_gain_ref, rows_of(h))
        pump(4)
        last = len(chunks) - 1
        for ci in range(max(1, last)):
            relayed(ci)
            all_arrived(ffn_groups[ci])
            if ci == min(1, last):
                pl.when(has_guest)(guest_gather)
                pump(6)
            ffn_chunk(ci, 0)
            if ci == 0:
                pump(5)
        pl.when(has_guest)(guest_forward)
        pump(7)
        pl.when(has_guest)(guest_ready)
        for ci in range(max(1, last)):
            pl.when(has_guest)(lambda: ffn_chunk(ci, 1))
            if ci == 0:
                pump(8)
        if last > 0:
            relayed(last)
            all_arrived(ffn_groups[last])
            ffn_chunk(last, 0)
            pump(9)
            pl.when(has_guest)(lambda: ffn_chunk(last, 1))
        pump(10)
        for i in range(len(ahead)):
            send_own(i)
        waiting = []

        def entry(valid, j, c, ready, hurry):
            @pl.when(valid)
            def _():
                ready()
                down_compute(j, c)

            if waiting:
                settle()
            waiting.append((valid, j, c))
            if hurry:
                settle()

        def settle():
            valid, j, c = waiting.pop()

            @pl.when(valid)
            def _():
                down_pass(j, c)

        for c in range(pieces):
            entry(True, f, c, lambda: None, False)
        for which in ("near", "far"):
            way, top = ways[which]
            for c in range(pieces):
                for step in range(1, top + 1):
                    m = down_at + c
                    relay(first_down + c, which, step)
                    ready = functools.partial(arrived, m, way, step)
                    j = f + step * (2 * way - 1)
                    entry(gets(m, way, step), j, c, ready, which == "far")
        if waiting:
            settle()

        @pl.when(has_guest)
        def _():
            sum_out[...] = down_total(1).astype(bf16)
            back_copy().start()

        second[...] = first_all[0, t].astype(f32) + down_total(0)

    @pl.when(outer)
    def _():
        back_copy().wait_recv()
        second[...] = first_all[0, t].astype(f32) + sum_in[...].astype(f32)

    ones = jnp.ones((8, width), f32)
    squares[0] = dot(ones, second[...] * second[...], 1, 1)
    for d in others:
        square_copy(d).start()
    for d in others:
        square_copy(d).wait_recv()
    whole = squares[0]
    for d in others:
        whole += squares[d]
    factor = lax.rsqrt(jnp.transpose(whole) / features + epsilon)[:, :1]
    result_ref[...] = (second[...] * factor * final_gain_ref[...]).astype(bf16)

    for m in range(total_messages):
        for step in range(1, steps_of(m) + 1):
            for way in (0, 1):
                @pl.when(gives(m, way, step))
                def _():
                    z_copy(m, way, step).wait_send()

                got = gets(m, way, step)
                if comes_whole(m, step):
                    got = jnp.logical_and(got, jnp.logical_not(gets_whole(way)))

                @pl.when(got)
                def _():
                    y_copy(m, way, step).wait_send()

                if comes_whole(m, step):
                    @pl.when(gives_whole(way))
                    def _():
                        e_copy(m, way, f).wait_send()
    gather_drain(0, token_at)
    for h in range(HALVES):
        for c in range(chips):
            sib_copy(h, c).wait_send()
        for e in beyond:
            far_copy(h, e).wait_send()
    for d in others:
        square_copy(d).wait_send()

    @pl.when(outer)
    def _():
        for h in range(HALVES):
            guest_copy(h).wait_send()

    def drain_down(r):
        for h in range(HALVES):
            gather_drain(ag_kind(r, h), first_at(r, h))
        for j in range(n):
            for c in range(pieces):
                p = (j * cols + c * dc) // width

                @pl.when(p % 2 != core)
                def _():
                    dd_copy(r, j, c).wait_send()

                for e in beyond:
                    @pl.when(jnp.logical_and(p % 2 == core, lax.rem(chip + e, chips) == p // 2))
                    def _():
                        dx_copy(r, j, c, e).wait_send()

    pl.when(inner)(lambda: drain_down(0))

    @pl.when(has_guest)
    def _():
        drain_down(1)
        back_copy().wait_send()


def body(
    sizes, tokens, attn_gain, w_query, w_key, w_value, w_low, w_lift, decay_bias, head_gain,
    w_out, ffn_gain, w_gate, w_up, w_down, final_gain,
):
    n, tp = sizes
    rows, width = tokens.shape
    bf16, f32 = jnp.bfloat16, jnp.float32
    units, keys, values = w_gate.shape[1], w_query.shape[1], w_value.shape[1]
    mix_width = 2 * keys + values
    chips = tp // 2
    vmem = pltpu.VMEM
    held = [vmem((n, w_query.shape[0], mix_width), bf16)]
    held += [vmem((n, *w.shape), bf16) for w in (w_out, w_gate, w_up, w_down)]
    pieces = w_down.shape[1] // down_columns(w_down.shape[1])
    messages = 4 + 2 * len(unit_chunks(units)) + pieces
    dma = pltpu.SemaphoreType.DMA
    anywhere = pl.BlockSpec(memory_space=pl.ANY)
    inside = pl.BlockSpec(memory_space=pltpu.VMEM)
    return pl.pallas_call(
        functools.partial(layer_kernel, sizes),
        name="layer",
        out_shape=jax.ShapeDtypeStruct((rows, width), bf16),
        in_specs=[anywhere] + [inside] * 7 + [anywhere] * 7,
        out_specs=inside,
        scratch_shapes=held + [
            vmem((tp, rows, width), bf16),
            vmem((2, rows, width * tp), bf16),
            vmem((rows, mix_width), bf16),
            vmem((rows, keys), f32),
            vmem((rows, values), bf16),
            vmem((keys // DK, DK, DV), f32),
            vmem((tp, rows, width), bf16),
            vmem((chips, rows, width), bf16),
            vmem((chips - 1, rows, width), bf16),
            vmem((2, tp, rows, width), bf16),
            vmem((2, rows, units), bf16),
            vmem((2, tp, rows, width), bf16),
            vmem((2, chips, rows, width), bf16),
            vmem((2, chips - 1, rows, width), bf16),
            vmem((rows, width), bf16),
            vmem((rows, width), bf16),
            vmem((rows, width), f32),
            vmem((tp, 8, rows), f32),
            dma((messages, 2, n)),
            dma((messages, 2, n)),
            dma((messages, 2, n)),
            dma((messages, 2, n)),
            dma((messages, 2)),
            dma((messages, 2)),
            dma((1 + 2 * HALVES, tp - 1)),
            dma((1 + 2 * HALVES, tp - 1)),
            dma((HALVES, tp - 1)),
            dma((HALVES, tp - 1)),
            dma((n * pieces, 2)),
            dma((n * pieces, 2)),
            dma((n * pieces, 2, chips - 1)),
            dma((n * pieces, 2, chips - 1)),
            dma((HALVES,)),
            dma((HALVES,)),
            dma,
            dma,
            dma((tp,)),
            dma((tp,)),
            dma((8,)),
        ],
        compiler_params=pltpu.CompilerParams(
            collective_id=0, has_side_effects=True, vmem_limit_bytes=63 * 1024 * 1024
        ),
    )(
        tokens, attn_gain[None], w_low.T, w_lift, decay_bias[None], head_gain[None],
        ffn_gain[None], final_gain[None], w_query, w_key, w_value, w_out, w_gate, w_up, w_down,
    )


def solution(mesh):
    sizes = (mesh.shape["fs"], mesh.shape["tp"])
    return jax.shard_map(
        functools.partial(body, sizes),
        mesh=mesh,
        in_specs=(
            P(("grp", "fs"), "tp"),
            P(),
            P("fs", "tp"),
            P("fs", "tp"),
            P("fs", "tp"),
            P(),
            P(None, "tp"),
            P("tp"),
            P(),
            P("tp", "fs"),
            P(),
            P("fs", "tp"),
            P("fs", "tp"),
            P("tp", "fs"),
            P("tp"),
        ),
        out_specs=P(("grp", "fs"), "tp"),
        check_vma=False,
    )
```

time: 232 us -> 187 us (0.81)
  Pallas kernels: 230 us -> 185 us
    pallas_call x1, Pallas kernels: 230 us -> 185 us  [body(): pl.pallas_call(functools.partial(layer_kernel, sizes), name='layer', out_...]
where the time goes in v1:
time: 187 us
  Pallas kernels  185 us (99%)
  local copies, waits for them, and re-layouts  1.87 us (1%)
    pallas_call x1, Pallas kernels, body(): pl.pallas_call(functools.partial(layer_kernel, sizes), name='layer', out_...  185 us

profile of v1, /device:TPU:0, one launch (start us, length us, event | category | flops | bytes accessed | tf_op | source)
XLA Modules:
  0.0 187.0 jit_solution(14067266071375931551)
XLA Ops:
  0.0 185.1 %layer.1 = bf16[512,512]{1,0:T(8,128)(2,1)} custom-call(bf16[512,512]{1,0:T(8,128)(2,1)} %tokens_ref.1, f32[1,2048]{1,0:T(1,128)} %bitcast.7, bf16[32,2048]{1,0:T(8,128)(2,1)} %bitcast.6, bf16[32,256]{1,0:T(8,128)(2,1)} %w_lift_ref.1, f32[1,256]{1,0:T(1,128)} %bitcast.10, f32[1,256]{1,0:T(1,128)} %bitcast.11, f32[1,2048]{1,0:T(1,128)} %bitcast.8, ...), custom_call_target="tpu_custom_call" | custom-call | tf_op jit(solution)/shard_map/layer/pallas_call | solution.py:867
  185.1 1.9 copy.17

commit v2 on v1

--- a/solution.py
+++ b/solution.py
@@ -33,6 +33,14 @@
 
 def down_columns(columns):
     return 2 * LANES if columns % (2 * LANES) == 0 else LANES
+
+
+def down_parts(columns):
+    if columns % (2 * LANES):
+        return [(0, columns)]
+    parts = [(at, 2 * LANES) for at in range(0, columns, 2 * LANES)]
+    at, size = parts.pop()
+    return parts + [(at, LANES), (at + LANES, LANES)]
 
 
 def layer_kernel(
@@ -82,6 +90,7 @@
     y_recv,
     e_send,
     e_recv,
+    e_last,
     ag_send,
     ag_recv,
     rs_send,
@@ -117,12 +126,17 @@
 
     messages = []
     column = 0
-    for w in (w_query_ref, w_key_ref, w_value_ref):
-        messages.append((w, g_mix, 0, column, w.shape[1]))
-        column += w.shape[1]
-    messages.append((w_out_ref, g_out, 0, 0, w_out_ref.shape[1]))
+    for w, parts in ((w_query_ref, 1), (w_key_ref, 1), (w_value_ref, 2)):
+        size = w.shape[1] // parts
+        for part in range(parts):
+            messages.append((w, g_mix, part * size, column, size))
+            column += size
+    qkv = range(len(messages))
+    size = down_columns(w_out_ref.shape[1])
+    for at in range(0, w_out_ref.shape[1], size):
+        messages.append((w_out_ref, g_out, at, at, size))
     n_mix = len(messages)
-    qkv, outs = range(3), range(3, 4)
+    outs = range(len(qkv), n_mix)
     chunks = unit_chunks(w_gate_ref.shape[1])
     ffn_groups = []
     for start, size in chunks:
@@ -130,13 +144,21 @@
         messages.append((w_gate_ref, g_gate, start, start, size))
         messages.append((w_up_ref, g_up, start, start, size))
     cols = w_down_ref.shape[1]
-    dc = down_columns(cols)
-    pieces = cols // dc
+    split = down_parts(cols)
+    pieces = len(split)
     down_at = len(messages)
-    for c in range(pieces):
-        messages.append((w_down_ref, g_down, c * dc, c * dc, dc))
+    for start, size in split:
+        messages.append((w_down_ref, g_down, start, start, size))
     down_groups = [(down_at + c,) for c in range(pieces)]
     total_messages = len(messages)
+    last_down = total_messages - 1
+    last_size = messages[last_down][4]
+    holders = [g_mix, g_out, g_gate, g_up, g_down]
+    groups = [tuple(qkv), tuple(outs)] + ffn_groups + down_groups
+    group_of = {m: i for i, group in enumerate(groups) for m in group}
+
+    def holder_of(m):
+        return [i for i, held in enumerate(holders) if held is messages[m][1]][0]
 
     def is_ffn(m):
         return m >= n_mix
@@ -171,31 +193,63 @@
     def toward(way):
         return f + 1 - 2 * way
 
+    def ring_copy(source, at, send, recv, way):
+        return pltpu.make_async_remote_copy(
+            source, at, send, recv, device_id=(g, toward(way), t), device_id_type=MESH
+        )
+
+    def place(m, owner, which):
+        w, held, start, column, columns = messages[m]
+        return held.at[owner, half_of(w, which), pl.ds(column, columns)]
+
+    def source_of(m, which):
+        w, held, start, column, columns = messages[m]
+        return w.at[half_of(w, which), pl.ds(start, columns)]
+
     def z_copy(m, way, step):
+        owner = f + (step - 1) * (2 * way - 1)
+        at = place(m, owner, g)
+        source = source_of(m, g) if step == 1 else at
+        return ring_copy(
+            source, at, z_send.at[holder_of(m), owner + way], z_recv.at[m, owner], way
+        )
+
+    def received(m, way, step):
+        owner = f + step * (2 * way - 1)
+        at = place(m, owner, g)
+        return ring_copy(at, at, z_send.at[holder_of(m), owner + way], z_recv.at[m, owner], way)
+
+    def e_copy(m, way, owner):
+        send = e_last.at[way] if m == last_down else e_send.at[holder_of(m)]
+        at = place(m, owner, 1 - g)
+        return ring_copy(source_of(m, 1 - g), at, send, e_recv.at[group_of[m], way], way)
+
+    def y_copy(m, way, step):
+        owner = f + step * (2 * way - 1)
+        at = place(m, owner, g)
+        return pltpu.make_async_remote_copy(
+            at, at, y_send.at[holder_of(m), owner], y_recv.at[group_of[m], owner],
+            device_id=(1 - g, f, t), device_id_type=MESH,
+        )
+
+    def bytes_of(i, owner):
+        m = groups[i][0]
         w, held, start, column, columns = messages[m]
-        owner = f + (step - 1) * (2 * way - 1)
-        half = half_of(w, g)
-        at = held.at[owner, half, pl.ds(column, columns)]
-        source = w.at[half, pl.ds(start, columns)] if step == 1 else at
+        if i < 2:
+            return held.at[owner, half_of(w, g), :]
+        if len(groups[i]) == 2:
+            return held.at[owner, :, pl.ds(column, columns)]
+        return place(m, owner, g)
+
+    def whole_here(i, way):
+        at = bytes_of(i, f + 2 * way - 1)
+        return ring_copy(at, at, e_last.at[way], e_recv.at[i, way], way)
+
+    def y_here(i, way, step):
+        owner = f + step * (2 * way - 1)
+        at = bytes_of(i, owner)
         return pltpu.make_async_remote_copy(
-            source, at, z_send.at[m, way, step], z_recv.at[m, way, step],
-            device_id=(g, toward(way), t), device_id_type=MESH,
-        )
-
-    def e_copy(m, way, owner):
-        w, held, start, column, columns = messages[m]
-        half = half_of(w, 1 - g)
-        at = held.at[owner, half, pl.ds(column, columns)]
-        return pltpu.make_async_remote_copy(
-            w.at[half, pl.ds(start, columns)], at, e_send.at[m, way], e_recv.at[m, way],
-            device_id=(g, toward(way), t), device_id_type=MESH,
-        )
-
-    def y_copy(m, way, step):
-        w, held, _, column, columns = messages[m]
-        at = held.at[f + step * (2 * way - 1), half_of(w, g), pl.ds(column, columns)]
-        return pltpu.make_async_remote_copy(
-            at, at, y_send.at[m, way, step], y_recv.at[m, way, step],
+            at, at, y_send.at[0, owner], y_recv.at[i, owner],
             device_id=(1 - g, f, t), device_id_type=MESH,
         )
 
@@ -211,10 +265,14 @@
         low, high = (1, n - 2) if is_ffn(m) else (0, n - 1)
         return jnp.logical_and(there, jnp.logical_and(to >= low, to <= high))
 
-    def gives_whole(way):
+    def gives_whole(m, way):
+        if m == last_down:
+            return gives(m, way, 1)
         return f == jnp.where(way == 0, 0, n - 1)
 
-    def gets_whole(way):
+    def gets_whole(m, way):
+        if m == last_down:
+            return gets(m, way, 1)
         return f == jnp.where(way == 0, 1, n - 2)
 
     def launch(group, way):
@@ -226,7 +284,7 @@
     def complete(group):
         for way in (0, 1):
             for m in group:
-                @pl.when(gives_whole(way))
+                @pl.when(gives_whole(m, way))
                 def _():
                     e_copy(m, way, f).start()
 
@@ -239,7 +297,7 @@
             def _():
                 received(m, way, step).wait_recv()
                 if comes_whole(m, step):
-                    @pl.when(jnp.logical_not(gets_whole(way)))
+                    @pl.when(jnp.logical_not(gets_whole(m, way)))
                     def _():
                         y_copy(m, way, step).start()
                 else:
@@ -250,35 +308,28 @@
                 def _():
                     z_copy(m, way, step + 1).start()
 
-    def received(m, way, step):
-        w, held, start, column, columns = messages[m]
-        at = held.at[f + step * (2 * way - 1), half_of(w, g), pl.ds(column, columns)]
-        return pltpu.make_async_remote_copy(
-            at, at, z_send.at[m, way, step], z_recv.at[m, way, step],
-            device_id=(g, toward(way), t), device_id_type=MESH,
-        )
-
-    def arrived(m, way, step):
+    def arrived(i, way, step):
+        m = groups[i][0]
         if comes_whole(m, step):
-            whole = gets_whole(way)
+            whole = gets_whole(m, way)
 
             @pl.when(whole)
             def _():
-                e_copy(m, way, f + 2 * way - 1).wait_recv()
+                whole_here(i, way).wait_recv()
 
             @pl.when(jnp.logical_not(whole))
             def _():
-                y_copy(m, way, step).wait_recv()
+                y_here(i, way, step).wait_recv()
         else:
-            y_copy(m, way, step).wait_recv()
-
-    def all_arrived(group):
-        for m in group:
-            for step in range(1, steps_of(m) + 1):
-                for way in (0, 1):
-                    @pl.when(gets(m, way, step))
-                    def _():
-                        arrived(m, way, step)
+            y_here(i, way, step).wait_recv()
+
+    def all_arrived(i):
+        m = groups[i][0]
+        for step in range(1, steps_of(m) + 1):
+            for way in (0, 1):
+                @pl.when(gets(m, way, step))
+                def _():
+                    arrived(i, way, step)
 
     def peer_of(e):
         return 2 * lax.rem(chip + e, chips) + core
@@ -292,7 +343,7 @@
         )
 
     def ag_copy(kind, slot, source, target, peer):
-        return tp_copy(source, target, ag_send.at[kind, slot], ag_recv.at[kind, slot], peer)
+        return tp_copy(source, target, ag_send.at[kind], ag_recv.at[kind, slot], peer)
 
     others = range(1, tp)
     beyond = range(1, chips)
@@ -314,9 +365,8 @@
             came = at(from_of(e) + 1 - 2 * core)
             ag_copy(kind, chips - 1 + e, came, came, sibling).wait_recv()
 
-    def gather_drain(kind, at):
-        for slot in range(tp - 1):
-            ag_copy(kind, slot, at(t), at(t), sibling).wait_send()
+    def gather_drain(kind, every):
+        ag_copy(kind, 0, every, every, sibling).wait_send()
 
     def rows_of(h):
         return pl.ds(h * (rows // HALVES), rows // HALVES)
@@ -332,7 +382,7 @@
 
     def square_copy(d):
         peer = lax.rem(t + d, tp)
-        return tp_copy(squares.at[0], squares.at[d], sq_send.at[d], sq_recv.at[d], peer)
+        return tp_copy(squares.at[0], squares.at[d], sq_send, sq_recv, peer)
 
     ahead = ffn_groups + down_groups
     ways = {"near": (near, n // 2 - 1), "far": (far, n - 2)}
@@ -364,20 +414,34 @@
         for act in plan.get(k, ()):
             act()
 
-    last_unit = len(ffn_groups) - 1
+    down_index = [len(ffn_groups) + c for c in range(len(down_groups))]
+
+    def down_near():
+        for i in down_index[1:]:
+            relay(i, "near")
+
+    def down_early():
+        for i in down_index[1:]:
+            relay(i, "far", 1)
+
+    def down_own():
+        for i in down_index:
+            send_own(i)
+
     plan = {
-        -1: [lambda: send_own(0), lambda: send_own(1)],
-        0: [lambda: relay(0, "near")],
+        -1: [lambda: send_own(0)],
+        0: [lambda: relay(0, "near"), lambda: send_own(1)],
         1: [lambda: relay(0, "far", 1)],
-        2: [lambda: send_own(2), lambda: relay(1, "far", 1)],
-        3: [lambda: relay(1, "near"), lambda: relay(0, "far"), lambda: send_own(3)],
-        4: [lambda: relay(2, "far", 1)],
-        5: [lambda: relay(2, "near"), lambda: send_own(4), lambda: relay(1, "far")],
-        6: [lambda: relay(3, "far", 1)],
-        7: [lambda: relay(2, "far")],
-        8: [lambda: relay(4, "far", 1), lambda: relay(3, "near")],
-        9: [lambda: relay(3, "far")],
-        10: [lambda: relay(4, "near")],
+        2: [lambda: relay(1, "near"), lambda: send_own(2), lambda: relay(0, "far")],
+        4: [lambda: relay(1, "far", 1)],
+        14: [lambda: relay(1, "far")],
+        5: [lambda: relay(2, "near"), down_own],
+        6: [lambda: relay(2, "far", 1)],
+        12: [lambda: relay(2, "far")],
+        7: [lambda: relay(3, "far", 1)],
+        8: [lambda: relay(3, "near"), down_early],
+        9: [down_near, lambda: complete(down_groups[-1])],
+        10: [lambda: relay(3, "far")],
     }
 
     def last_step(way):
@@ -395,18 +459,21 @@
     @pl.when(outer)
     def _():
         complete(qkv)
-        for group in ffn_groups:
+        for group in ffn_groups[:-1]:
             for way in (0, 1):
                 launch(group, way)
-            if group != ffn_groups[-1]:
-                complete(group)
+        for group in ffn_groups[:-1]:
+            complete(group)
+        for way in (0, 1):
+            launch(ffn_groups[-1], way)
 
     gather_out(0, tokens_ref, token_at)
     locals_ = [pltpu.make_async_copy(tokens_ref, rows_all.at[t], local_sem.at[0])]
     own = [messages[m] for m in range(n_mix)]
     for index, (w, held, start, column, columns) in enumerate(own):
         at = held.at[f, :, pl.ds(column, columns)]
-        locals_.append(pltpu.make_async_copy(w, at, local_sem.at[1 + index]))
+        source = w.at[:, pl.ds(start, columns)]
+        locals_.append(pltpu.make_async_copy(source, at, local_sem.at[1 + index]))
     inner_locals = []
     for index, (w, held) in enumerate(((w_gate_ref, g_gate), (w_up_ref, g_up), (w_down_ref, g_down))):
         inner_locals.append(pltpu.make_async_copy(w, held.at[f], local_sem.at[1 + n_mix + index]))
@@ -463,7 +530,7 @@
     lifted = jnp.dot(low_rank.astype(bf16), w_lift_ref[...], preferred_element_type=f32)
     log_decay[...] = jax.nn.log_sigmoid(lifted + decay_bias_ref[...]) / 16.0
 
-    all_arrived(qkv)
+    all_arrived(0)
     tick(outs, far, 1)
     mix_block = 2 * LANES if mix_rows.shape[1] % (2 * LANES) == 0 else LANES
 
@@ -481,47 +548,55 @@
     at_row = lax.broadcasted_iota(jnp.int32, (BLOCK, BLOCK), 0)
     at_col = lax.broadcasted_iota(jnp.int32, (BLOCK, BLOCK), 1)
     causal = at_row >= at_col
-    lower = causal.astype(f32)
+    lower = causal.astype(bf16)
 
     def dot(a, b, ca, cb):
         return lax.dot_general(
             a, b, (((ca,), (cb,)), ((), ())), precision=highest, preferred_element_type=f32
         )
 
+    def short_dot(a, b, ca, cb):
+        a, b = a.astype(bf16), b.astype(bf16)
+        return lax.dot_general(a, b, (((ca,), (cb,)), ((), ())), preferred_element_type=f32)
+
     state[...] = jnp.zeros_like(state)
 
-    def block_step(block, carry):
-        here = pl.ds(pl.multiple_of(block * BLOCK, BLOCK), BLOCK)
+    def block_step(here):
+        decays = log_decay[here, :]
+        high = decays.astype(bf16)
+        low = decays - high.astype(f32)
+        sums = short_dot(lower, high, 1, 0) + short_dot(lower, low, 1, 0)
         for h in range(heads):
             query = mix_rows[here, pl.ds(h * DK, DK)].astype(f32) * DK ** (-0.5)
             key = mix_rows[here, pl.ds((heads + h) * DK, DK)].astype(f32)
-            value = mix_rows[here, pl.ds(2 * heads * DK + h * DV, DV)].astype(f32)
-            cum = dot(lower, log_decay[here, pl.ds(h * DK, DK)], 1, 0)
+            value = mix_rows[here, pl.ds(2 * heads * DK + h * DV, DV)]
+            cum = sums[:, h * DK : (h + 1) * DK]
             last = cum[BLOCK - 1 :, :]
-            query_dec = query * jnp.exp(cum)
+            query_dec = (query * jnp.exp(cum)).astype(bf16)
             key_dec = key * jnp.exp(-cum)
-            scores = jnp.where(causal, dot(query_dec, key_dec, 1, 1), 0.0)
+            scores = jnp.where(causal, short_dot(query_dec, key_dec, 1, 1), 0.0)
             held = state[h]
-            out = dot(scores, value, 1, 0) + dot(query_dec, held, 1, 0)
-            decay = jnp.transpose(jnp.broadcast_to(jnp.exp(last), (DK, DK)))
-            decay = jnp.concatenate([decay] * (DV // DK), axis=1)
-            state[h] = decay * held + dot(key * jnp.exp(last - cum), value, 0, 0)
+            out = short_dot(scores, value, 1, 0) + short_dot(query_dec, held, 1, 1)
+            state[h] = jnp.exp(last) * held + short_dot(value, key * jnp.exp(last - cum), 0, 0)
             factor = lax.rsqrt(jnp.mean(out * out, axis=1, keepdims=True) + epsilon)
             mixed[here, pl.ds(h * DV, DV)] = (out * factor * head_gain_ref[...]).astype(bf16)
-        return carry
+
+    def gla(start, stop):
+        for block in range(start, stop):
+            block_step(pl.ds(block * BLOCK, BLOCK))
 
     blocks = rows // BLOCK
-    lax.fori_loop(0, blocks // 2, block_step, 0)
+    gla(0, blocks // 2)
     pl.when(inner)(lambda: pump(1))
-    lax.fori_loop(blocks // 2, blocks, block_step, 0)
     tick(outs, far, n - 1)
-    all_arrived(outs)
+    gla(blocks // 2, blocks)
+    all_arrived(1)
 
     def block_place(place, size):
         return place // width, pl.ds(pl.multiple_of(lax.rem(place, width), LANES), size)
 
     def rs_copy(h, slot, source, target, peer):
-        return tp_copy(source, target, rs_send.at[h, slot], rs_recv.at[h, slot], peer)
+        return tp_copy(source, target, rs_send.at[h], rs_recv.at[h, slot], peer)
 
     def sib_copy(h, c):
         return rs_copy(
@@ -621,7 +696,7 @@
             normalize(first_all.at[1], 1, ffn_gain_ref, rows_of(h))
 
     def place_of(j, c):
-        p, part = block_place(j * cols + c * dc, dc)
+        p, part = block_place(j * cols + split[c][0], split[c][1])
         return p, part
 
     def dd_copy(r, j, c):
@@ -639,211 +714,259 @@
             2 * (p // 2) + core,
         )
 
-    def sets(act):
+    def down_compute(j, c, r):
+        p, part = place_of(j, c)
+        terms = jnp.dot(hidden[r], g_down[j, :, pl.ds(*split[c])], preferred_element_type=f32)
+        partial_down[r, p, :, part] = terms.astype(bf16)
+
+        @pl.when(lax.rem(p, 2) != core)
+        def _():
+            dd_copy(r, j, c).start()
+
+    def down_pass(j, c, r):
+        p, part = place_of(j, c)
+
+        @pl.when(jnp.logical_and(lax.rem(p, 2) == core, p // 2 != chip))
+        def _():
+            dd_copy(r, j, c).wait_recv()
+            pair = partial_down[r, p, :, part].astype(f32)
+            pair += sib_down[r, p // 2, :, part].astype(f32)
+            partial_down[r, p, :, part] = pair.astype(bf16)
+            for e in beyond:
+                @pl.when(lax.rem(chip + e, chips) == p // 2)
+                def _():
+                    dx_copy(r, j, c, e).start()
+
+    def each_set(low, act):
         def one(i, carry):
             act(guests - i)
             return carry
 
-        lax.fori_loop(0, 1 + guests, one, 0)
-
-    def down_compute(j, c):
+        lax.fori_loop(0, guests + 1 - low, one, 0)
+
+    squares[0] = jnp.zeros((8, rows), f32)
+
+    def settle(part, values):
+        second[:, part] = values
+        squares[0] += dot(jnp.ones((8, part.size), f32), values * values, 1, 1)
+
+    def back_copy(j, c):
+        part = place_of(j, c)[1]
+        k = j * pieces + c
+        return pltpu.make_async_remote_copy(
+            sum_out.at[:, part], sum_in.at[:, part], back_send, back_recv.at[k],
+            device_id=(g, guest_plane, t), device_id_type=MESH,
+        )
+
+    def down_total(j, c, r):
         p, part = place_of(j, c)
 
-        def act(r):
-            terms = jnp.dot(hidden[r], g_down[j, :, pl.ds(c * dc, dc)], preferred_element_type=f32)
-            partial_down[r, p, :, part] = terms.astype(bf16)
-
-            @pl.when(lax.rem(p, 2) != core)
-            def _():
-                dd_copy(r, j, c).start()
-
-        sets(act)
-
-    def down_pass(j, c):
-        p, part = place_of(j, c)
-
-        @pl.when(jnp.logical_and(lax.rem(p, 2) == core, p // 2 != chip))
+        @pl.when(p == t)
         def _():
-            def act(r):
+            def whole_of(r):
                 dd_copy(r, j, c).wait_recv()
-                pair = partial_down[r, p, :, part].astype(f32)
-                pair += sib_down[r, p // 2, :, part].astype(f32)
-                partial_down[r, p, :, part] = pair.astype(bf16)
                 for e in beyond:
-                    @pl.when(lax.rem(chip + e, chips) == p // 2)
+                    dx_copy(r, j, c, e).wait_recv()
+                total = partial_down[r, t, :, part].astype(f32)
+                total += sib_down[r, chip, :, part].astype(f32)
+                for e in beyond:
+                    total += far_down[r, e - 1, :, part].astype(f32)
+                return total
+
+            if r:
+                sum_out[:, part] = whole_of(r).astype(bf16)
+                back_copy(j, c).start()
+            else:
+                settle(part, first_all[0, t, :, part].astype(f32) + whole_of(r))
+
+    def drain_sends(which):
+        for i in which:
+            m = [m for m in range(total_messages) if holder_of(m) == i][0]
+            held, w = holders[i], messages[m][0]
+            width_of = held.shape[2]
+            direct = width_of - last_size if i == 4 else width_of
+            for step in range(1, steps_of(m) + 1):
+                for way in (0, 1):
+                    owner = f + (step - 1) * (2 * way - 1)
+
+                    @pl.when(gives(m, way, step))
                     def _():
-                        dx_copy(r, j, c, e).start()
-
-            sets(act)
-
-    def down_total(r):
+                        at = held.at[owner, half_of(w, g), :]
+                        ring_copy(at, at, z_send.at[i, owner + way], z_recv.at[m, owner], way).wait_send()
+
+                    got = gets(m, way, step)
+                    size = width_of
+                    if comes_whole(m, step):
+                        got = jnp.logical_and(got, f != jnp.where(way == 0, 1, n - 2))
+                        size = direct
+                    came = f + step * (2 * way - 1)
+                    if size:
+                        @pl.when(got)
+                        def _():
+                            at = held.at[came, half_of(w, g), pl.ds(0, size)]
+                            ring_copy(at, at, y_send.at[i, came], z_recv.at[m, came], way).wait_send()
+
+                    if comes_whole(m, step) and direct:
+                        @pl.when(f == jnp.where(way == 0, 0, n - 1))
+                        def _():
+                            at = held.at[f, half_of(w, g), pl.ds(0, direct)]
+                            ring_copy(at, at, e_send.at[i], e_recv.at[0, way], way).wait_send()
+
+                    if i == 4 and step == 1:
+                        @pl.when(gives(last_down, way, 1))
+                        def _():
+                            e_copy(last_down, way, f).wait_send()
+
+    def drain_mixer():
+        gather_drain(0, rows_all.at[pl.ds(0, tp - 1)])
+        for h in range(HALVES):
+            every = partial_out.at[pl.ds(0, tp - 1), rows_of(h)]
+            rs_copy(h, 0, every, every, sibling).wait_send()
+
+    def drain_rows(r):
+        for h in range(HALVES):
+            gather_drain(ag_kind(r, h), first_all.at[r, pl.ds(0, tp - 1), rows_of(h)])
+
+    def drain_down(r):
         for j in range(n):
             for c in range(pieces):
-                @pl.when((j * cols + c * dc) // width == t)
+                p = (j * cols + split[c][0]) // width
+
+                @pl.when(p % 2 != core)
                 def _():
-                    dd_copy(r, j, c).wait_recv()
-                    for e in beyond:
-                        dx_copy(r, j, c, e).wait_recv()
-        total = partial_down[r, t].astype(f32) + sib_down[r, chip].astype(f32)
-        for e in beyond:
-            total += far_down[r, e - 1].astype(f32)
-        return total
-
-    def back_copy():
-        return pltpu.make_async_remote_copy(
-            sum_out, sum_in, back_send, back_recv,
-            device_id=(g, guest_plane, t), device_id_type=MESH,
-        )
+                    dd_copy(r, j, c).wait_send()
+
+                for e in beyond:
+                    @pl.when(jnp.logical_and(p % 2 == core, lax.rem(chip + e, chips) == p // 2))
+                    def _():
+                        dx_copy(r, j, c, e).wait_send()
 
     @pl.when(inner)
     def _():
-        pump(3)
+        pump(4)
         for h in range(HALVES):
             gather_forward(ag_kind(0, h), first_at(0, h))
         for h in range(HALVES):
             gather_wait(ag_kind(0, h), first_at(0, h))
             normalize(first_all.at[0], 0, ffn_gain_ref, rows_of(h))
-        pump(4)
         last = len(chunks) - 1
-        for ci in range(max(1, last)):
-            relayed(ci)
-            all_arrived(ffn_groups[ci])
-            if ci == min(1, last):
-                pl.when(has_guest)(guest_gather)
-                pump(6)
-            ffn_chunk(ci, 0)
-            if ci == 0:
-                pump(5)
+        relayed(0)
+        all_arrived(2)
+        pump(14)
+        ffn_chunk(0, 0)
+        pump(5)
+        pump(6)
+        pl.when(has_guest)(guest_gather)
+        if last > 1:
+            relayed(1)
+            all_arrived(3)
+            ffn_chunk(1, 0)
         pl.when(has_guest)(guest_forward)
+        pump(12)
+        pl.when(has_guest)(guest_ready)
+        pl.when(has_guest)(lambda: ffn_chunk(0, 1))
         pump(7)
-        pl.when(has_guest)(guest_ready)
-        for ci in range(max(1, last)):
-            pl.when(has_guest)(lambda: ffn_chunk(ci, 1))
-            if ci == 0:
-                pump(8)
+        if last > 1:
+            pl.when(has_guest)(lambda: ffn_chunk(1, 1))
+        pump(8)
         if last > 0:
             relayed(last)
-            all_arrived(ffn_groups[last])
+            all_arrived(2 + last)
             ffn_chunk(last, 0)
-            pump(9)
+        pump(9)
+        for c in range(pieces):
+            down_compute(f, c, 0)
+        if last > 0:
             pl.when(has_guest)(lambda: ffn_chunk(last, 1))
-        pump(10)
         for i in range(len(ahead)):
             send_own(i)
-        waiting = []
-
-        def entry(valid, j, c, ready, hurry):
+        pump(10)
+        for c in range(pieces):
+            down_pass(f, c, 0)
+            pl.when(has_guest)(lambda: down_compute(f, c, 1))
+        done = [(True, f, c) for c in range(pieces)]
+        waiting = [lambda: [down_pass(f, c, 1) for c in range(pieces)] and None]
+        waiting = [functools.partial(pl.when(has_guest), waiting[0])]
+
+        def entry(which, step, c):
+            way = ways[which][0]
+            m, j = down_at + c, f + step * (2 * way - 1)
+            valid = gets(m, way, step)
+            relay(first_down + c, which, step)
+            if which == "near":
+                relay(first_down + c + 1, "far")
+            if (which, step, c) == order[-1]:
+                drain_sends(range(4))
+                drain_mixer()
+                drain_rows(0)
+                pl.when(has_guest)(lambda: drain_rows(1))
+
             @pl.when(valid)
             def _():
-                ready()
-                down_compute(j, c)
+                arrived(group_of[m], way, step)
+                each_set(0, lambda r: down_compute(j, c, r))
 
             if waiting:
-                settle()
-            waiting.append((valid, j, c))
-            if hurry:
-                settle()
-
-        def settle():
-            valid, j, c = waiting.pop()
-
-            @pl.when(valid)
-            def _():
-                down_pass(j, c)
-
+                waiting.pop()()
+            done.append((valid, j, c))
+            send = lambda: pl.when(valid)(lambda: each_set(0, lambda r: down_pass(j, c, r)))
+            waiting.append(send)
+
+        final = n - 2
+        order = [("far", step, c) for c in range(pieces - 1) for step in range(1, final)]
         for c in range(pieces):
-            entry(True, f, c, lambda: None, False)
-        for which in ("near", "far"):
-            way, top = ways[which]
-            for c in range(pieces):
-                for step in range(1, top + 1):
-                    m = down_at + c
-                    relay(first_down + c, which, step)
-                    ready = functools.partial(arrived, m, way, step)
-                    j = f + step * (2 * way - 1)
-                    entry(gets(m, way, step), j, c, ready, which == "far")
-        if waiting:
-            settle()
-
-        @pl.when(has_guest)
-        def _():
-            sum_out[...] = down_total(1).astype(bf16)
-            back_copy().start()
-
-        second[...] = first_all[0, t].astype(f32) + down_total(0)
+            order += [("near", step, c) for step in range(1, ways["near"][1] + 1)]
+            if c == pieces - 1:
+                order += [("far", step, c) for step in range(1, final)]
+            order += [("far", final, c)]
+        for which, step, c in order:
+            entry(which, step, c)
+        waiting.pop()()
+        for r in (1, 0):
+            for valid, j, c in done:
+                guard = jnp.logical_and(valid, has_guest) if r else valid
+                pl.when(guard)(lambda: down_total(j, c, r))
 
     @pl.when(outer)
     def _():
-        back_copy().wait_recv()
-        second[...] = first_all[0, t].astype(f32) + sum_in[...].astype(f32)
-
-    ones = jnp.ones((8, width), f32)
-    squares[0] = dot(ones, second[...] * second[...], 1, 1)
+        drain_sends(range(5))
+        drain_mixer()
+        for h in range(HALVES):
+            guest_copy(h).wait_send()
+        for j in range(n):
+            for c in range(pieces):
+                p, part = place_of(j, c)
+
+                @pl.when(p == t)
+                def _():
+                    back_copy(j, c).wait_recv()
+                    total = sum_in[:, part].astype(f32)
+                    settle(part, first_all[0, t, :, part].astype(f32) + total)
+
     for d in others:
         square_copy(d).start()
-    for d in others:
-        square_copy(d).wait_recv()
+    sent, heard = squares.at[pl.ds(0, tp - 1)], squares.at[pl.ds(1, tp - 1)]
+    tp_copy(sent, heard, sq_send, sq_recv, sibling).wait_recv()
     whole = squares[0]
     for d in others:
         whole += squares[d]
     factor = lax.rsqrt(jnp.transpose(whole) / features + epsilon)[:, :1]
     result_ref[...] = (second[...] * factor * final_gain_ref[...]).astype(bf16)
 
-    for m in range(total_messages):
-        for step in range(1, steps_of(m) + 1):
-            for way in (0, 1):
-                @pl.when(gives(m, way, step))
-                def _():
-                    z_copy(m, way, step).wait_send()
-
-                got = gets(m, way, step)
-                if comes_whole(m, step):
-                    got = jnp.logical_and(got, jnp.logical_not(gets_whole(way)))
-
-                @pl.when(got)
-                def _():
-                    y_copy(m, way, step).wait_send()
-
-                if comes_whole(m, step):
-                    @pl.when(gives_whole(way))
-                    def _():
-                        e_copy(m, way, f).wait_send()
-    gather_drain(0, token_at)
-    for h in range(HALVES):
-        for c in range(chips):
-            sib_copy(h, c).wait_send()
-        for e in beyond:
-            far_copy(h, e).wait_send()
-    for d in others:
-        square_copy(d).wait_send()
-
-    @pl.when(outer)
+    tp_copy(sent, heard, sq_send, sq_recv, sibling).wait_send()
+
+    @pl.when(inner)
     def _():
-        for h in range(HALVES):
-            guest_copy(h).wait_send()
-
-    def drain_down(r):
-        for h in range(HALVES):
-            gather_drain(ag_kind(r, h), first_at(r, h))
-        for j in range(n):
-            for c in range(pieces):
-                p = (j * cols + c * dc) // width
-
-                @pl.when(p % 2 != core)
-                def _():
-                    dd_copy(r, j, c).wait_send()
-
-                for e in beyond:
-                    @pl.when(jnp.logical_and(p % 2 == core, lax.rem(chip + e, chips) == p // 2))
-                    def _():
-                        dx_copy(r, j, c, e).wait_send()
-
-    pl.when(inner)(lambda: drain_down(0))
+        drain_sends((4,))
+        drain_down(0)
 
     @pl.when(has_guest)
     def _():
         drain_down(1)
-        back_copy().wait_send()
+        pltpu.make_async_remote_copy(
+            sum_out, sum_in, back_send, back_recv.at[0],
+            device_id=(g, guest_plane, t), device_id_type=MESH,
+        ).wait_send()
 
 
 def body(
@@ -859,8 +982,10 @@
     vmem = pltpu.VMEM
     held = [vmem((n, w_query.shape[0], mix_width), bf16)]
     held += [vmem((n, *w.shape), bf16) for w in (w_out, w_gate, w_up, w_down)]
-    pieces = w_down.shape[1] // down_columns(w_down.shape[1])
-    messages = 4 + 2 * len(unit_chunks(units)) + pieces
+    pieces = len(down_parts(w_down.shape[1]))
+    messages = 4 + w_out.shape[1] // down_columns(w_out.shape[1])
+    messages += 2 * len(unit_chunks(units)) + pieces
+    groups = 2 + len(unit_chunks(units)) + pieces
     dma = pltpu.SemaphoreType.DMA
     anywhere = pl.BlockSpec(memory_space=pl.ANY)
     inside = pl.BlockSpec(memory_space=pltpu.VMEM)
@@ -876,7 +1001,7 @@
             vmem((rows, mix_width), bf16),
             vmem((rows, keys), f32),
             vmem((rows, values), bf16),
-            vmem((keys // DK, DK, DV), f32),
+            vmem((keys // DK, DV, DK), f32),
             vmem((tp, rows, width), bf16),
             vmem((chips, rows, width), bf16),
             vmem((chips - 1, rows, width), bf16),
@@ -889,15 +1014,16 @@
             vmem((rows, width), bf16),
             vmem((rows, width), f32),
             vmem((tp, 8, rows), f32),
-            dma((messages, 2, n)),
-            dma((messages, 2, n)),
-            dma((messages, 2, n)),
-            dma((messages, 2, n)),
-            dma((messages, 2)),
-            dma((messages, 2)),
+            dma((5, n + 1)),
+            dma((messages, n)),
+            dma((5, n)),
+            dma((groups, n)),
+            dma((5,)),
+            dma((groups, 2)),
+            dma((2,)),
+            dma((1 + 2 * HALVES,)),
             dma((1 + 2 * HALVES, tp - 1)),
-            dma((1 + 2 * HALVES, tp - 1)),
-            dma((HALVES, tp - 1)),
+            dma((HALVES,)),
             dma((HALVES, tp - 1)),
             dma((n * pieces, 2)),
             dma((n * pieces, 2)),
@@ -906,10 +1032,10 @@
             dma((HALVES,)),
             dma((HALVES,)),
             dma,
+            dma((n * pieces,)),
             dma,
-            dma((tp,)),
-            dma((tp,)),
-            dma((8,)),
+            dma,
+            dma((12,)),
         ],
         compiler_params=pltpu.CompilerParams(
             collective_id=0, has_side_effects=True, vmem_limit_bytes=63 * 1024 * 1024

time: 187 us -> 169 us (0.904)
  Pallas kernels: 185 us -> 167 us
    pallas_call x1, Pallas kernels: 185 us -> 167 us  [body(): pl.pallas_call(functools.partial(layer_kernel, sizes), name='layer', out_...]
where the time goes in v2:
time: 169 us
  Pallas kernels  167 us (99%)
  local copies, waits for them, and re-layouts  1.87 us (1%)
    pallas_call x1, Pallas kernels, body(): pl.pallas_call(functools.partial(layer_kernel, sizes), name='layer', out_...  167 us

profile of v2, /device:TPU:0, one launch (start us, length us, event | category | flops | bytes accessed | tf_op | source)
XLA Modules:
  0.0 169.0 jit_solution(9287050385363308107)
XLA Ops:
  0.0 167.1 %layer.1 = bf16[512,512]{1,0:T(8,128)(2,1)} custom-call(bf16[512,512]{1,0:T(8,128)(2,1)} %tokens_ref.1, f32[1,2048]{1,0:T(1,128)} %bitcast.7, bf16[32,2048]{1,0:T(8,128)(2,1)} %bitcast.6, bf16[32,256]{1,0:T(8,128)(2,1)} %w_lift_ref.1, f32[1,256]{1,0:T(1,128)} %bitcast.10, f32[1,256]{1,0:T(1,128)} %bitcast.11, f32[1,2048]{1,0:T(1,128)} %bitcast.8, ...), custom_call_target="tpu_custom_call" | custom-call | tf_op jit(solution)/shard_map/layer/pallas_call | solution.py:992
  167.1 1.9 %copy.17 = bf16[512,512]{1,0:T(8,128)(2,1)} copy(bf16[512,512]{1,0:T(8,128)(2,1)} %layer.1) | data formatting | bytes 1048576

commit v3 on v2

--- a/solution.py
+++ b/solution.py
@@ -699,18 +699,23 @@
         p, part = block_place(j * cols + split[c][0], split[c][1])
         return p, part
 
+    per = max(1, width // cols)
+
+    def slot_of(j, c):
+        return lax.rem(j, per) * pieces + c
+
     def dd_copy(r, j, c):
         p, part = place_of(j, c)
         return tp_copy(
             partial_down.at[r, p, :, part], sib_down.at[r, p // 2, :, part],
-            dd_send.at[j * pieces + c, r], dd_recv.at[j * pieces + c, r], sibling,
+            dd_send.at[r], dd_recv.at[j * pieces + c, r], sibling,
         )
 
     def dx_copy(r, j, c, e):
         p, part = place_of(j, c)
         return tp_copy(
             partial_down.at[r, p, :, part], far_down.at[r, e - 1, :, part],
-            dx_send.at[j * pieces + c, r, e - 1], dx_recv.at[j * pieces + c, r, e - 1],
+            dx_send.at[r], dx_recv.at[slot_of(j, c), r, e - 1],
             2 * (p // 2) + core,
         )
 
@@ -752,7 +757,7 @@
 
     def back_copy(j, c):
         part = place_of(j, c)[1]
-        k = j * pieces + c
+        k = slot_of(j, c)
         return pltpu.make_async_remote_copy(
             sum_out.at[:, part], sum_in.at[:, part], back_send, back_recv.at[k],
             device_id=(g, guest_plane, t), device_id_type=MESH,
@@ -828,18 +833,11 @@
             gather_drain(ag_kind(r, h), first_all.at[r, pl.ds(0, tp - 1), rows_of(h)])
 
     def drain_down(r):
-        for j in range(n):
-            for c in range(pieces):
-                p = (j * cols + split[c][0]) // width
-
-                @pl.when(p % 2 != core)
-                def _():
-                    dd_copy(r, j, c).wait_send()
-
-                for e in beyond:
-                    @pl.when(jnp.logical_and(p % 2 == core, lax.rem(chip + e, chips) == p // 2))
-                    def _():
-                        dx_copy(r, j, c, e).wait_send()
+        every = partial_down.at[r, pl.ds(0, chips)]
+        tp_copy(every, every, dd_send.at[r], dd_recv.at[0, r], sibling).wait_send()
+        if chips > 1:
+            every = partial_down.at[r, pl.ds(0, chips - 1)]
+            tp_copy(every, every, dx_send.at[r], dd_recv.at[0, r], sibling).wait_send()
 
     @pl.when(inner)
     def _():
@@ -895,7 +893,7 @@
             relay(first_down + c, which, step)
             if which == "near":
                 relay(first_down + c + 1, "far")
-            if (which, step, c) == order[-1]:
+            if (which, step, c) == ("far", final, 0):
                 drain_sends(range(4))
                 drain_mixer()
                 drain_rows(0)
@@ -909,7 +907,12 @@
             if waiting:
                 waiting.pop()()
             done.append((valid, j, c))
-            send = lambda: pl.when(valid)(lambda: each_set(0, lambda r: down_pass(j, c, r)))
+            if order.index((which, step, c)) < order.index(("far", final, 0)):
+                send = lambda: pl.when(valid)(lambda: each_set(0, lambda r: down_pass(j, c, r)))
+            else:
+                guest = jnp.logical_and(valid, has_guest)
+                send = lambda: pl.when(guest)(lambda: down_pass(j, c, 1))
+                owed.append(lambda: pl.when(valid)(lambda: down_pass(j, c, 0)))
             waiting.append(send)
 
         final = n - 2
@@ -919,9 +922,12 @@
             if c == pieces - 1:
                 order += [("far", step, c) for step in range(1, final)]
             order += [("far", final, c)]
+        owed = []
         for which, step, c in order:
             entry(which, step, c)
         waiting.pop()()
+        for send in owed:
+            send()
         for r in (1, 0):
             for valid, j, c in done:
                 guard = jnp.logical_and(valid, has_guest) if r else valid
@@ -983,6 +989,7 @@
     held = [vmem((n, w_query.shape[0], mix_width), bf16)]
     held += [vmem((n, *w.shape), bf16) for w in (w_out, w_gate, w_up, w_down)]
     pieces = len(down_parts(w_down.shape[1]))
+    per = max(1, width // w_down.shape[1])
     messages = 4 + w_out.shape[1] // down_columns(w_out.shape[1])
     messages += 2 * len(unit_chunks(units)) + pieces
     groups = 2 + len(unit_chunks(units)) + pieces
@@ -1025,14 +1032,14 @@
             dma((1 + 2 * HALVES, tp - 1)),
             dma((HALVES,)),
             dma((HALVES, tp - 1)),
+            dma((2,)),
             dma((n * pieces, 2)),
-            dma((n * pieces, 2)),
-            dma((n * pieces, 2, chips - 1)),
-            dma((n * pieces, 2, chips - 1)),
+            dma((2,)),
+            dma((per * pieces, 2, chips - 1)),
             dma((HALVES,)),
             dma((HALVES,)),
             dma,
-            dma((n * pieces,)),
+            dma((per * pieces,)),
             dma,
             dma,
             dma((12,)),

time: 169 us -> 168 us (level)
  no operation moved by 1% of the time
where the time goes in v3:
time: 168 us
  Pallas kernels  166 us (99%)
  local copies, waits for them, and re-layouts  1.87 us (1%)
    pallas_call x1, Pallas kernels, body(): pl.pallas_call(functools.partial(layer_kernel, sizes), name='layer', out_...  166 us

profile of v3, /device:TPU:0, one launch (start us, length us, event | category | flops | bytes accessed | tf_op | source)
XLA Modules:
  0.0 168.3 jit_solution(16993592163709465001)
XLA Ops:
  0.0 166.4 %layer.1 = bf16[512,512]{1,0:T(8,128)(2,1)} custom-call(bf16[512,512]{1,0:T(8,128)(2,1)} %tokens_ref.1, f32[1,2048]{1,0:T(1,128)} %bitcast.7, bf16[32,2048]{1,0:T(8,128)(2,1)} %bitcast.6, bf16[32,256]{1,0:T(8,128)(2,1)} %w_lift_ref.1, f32[1,256]{1,0:T(1,128)} %bitcast.10, f32[1,256]{1,0:T(1,128)} %bitcast.11, f32[1,2048]{1,0:T(1,128)} %bitcast.8, ...), custom_call_target="tpu_custom_call" | custom-call | tf_op jit(solution)/shard_map/layer/pallas_call | solution.py:999
  166.4 1.9 %copy.17 = bf16[512,512]{1,0:T(8,128)(2,1)} copy(bf16[512,512]{1,0:T(8,128)(2,1)} %layer.1) | data formatting | bytes 1048576
